TPU v7x, 32 devices: a whole 2x2x4 slice. The times are simulated.
32 devices in a mesh: grp: 2 (over x), sp: 4 (over y, core), tp: 4 (over z).
Axes of the slice: x: 2, y: 2, z: 4, core: 2. Of those that a mesh axis runs over, the one named last changes fastest.
Arguments:
- layer_input: bfloat16 [8, 1024, 2048], P(('grp', 'tp'), 'sp'), parts along dimension 0, may hold values from -6 to 6
- norm_gain: bfloat16 [2048], replicated, may hold values from 0.099609375 to 1.8984375
- key_weight: bfloat16 [2048, 1024], replicated, may hold values from -0.125 to 0.125
- value_weight: bfloat16 [2048, 1024], replicated, may hold values from -0.125 to 0.125
- input_gate_weight: bfloat16 [2048, 8], replicated, may hold values from -0.125 to 0.125
- forget_gate_weight: bfloat16 [2048, 8], replicated, may hold values from -0.125 to 0.125
- conv_weight: float32 [4, 1024], replicated, may hold values from -3 to 3
- input_shift: float32 [8, 8, 1024], P(('grp', 'sp'), 'tp'), parts along dimension 0, may hold values from -4 to 302
- forget_shift: float32 [8, 8, 1024], P(('grp', 'sp'), 'tp'), parts along dimension 0, may hold values from 0 to 10.1
- new_query: bfloat16 [8, 8, 128], P(('grp', 'sp'), 'tp'), parts along dimension 0, may hold values from 0.1 to 2
- new_key: bfloat16 [8, 8, 128], P(('grp', 'sp'), 'tp'), parts along dimension 0, may hold values from -6 to 6
- new_value: bfloat16 [8, 8, 128], P(('grp', 'sp'), 'tp'), parts along dimension 0, may hold values from -6 to 6
- new_input: float32 [8, 8], P(('grp', 'sp'), 'tp'), parts along dimension 0, may hold values from 2 to 6
- new_forget: float32 [8, 8], P(('grp', 'sp'), 'tp'), parts along dimension 0, may hold values from -1 to 3
Outputs:
- key_cache: bfloat16 [8, 8, 1024, 128], P(('grp', 'sp'), 'tp'), parts along dimension 0
- value_cache: bfloat16 [8, 8, 1024, 128], P(('grp', 'sp'), 'tp'), parts along dimension 0
- weight_cache: float32 [8, 8, 1024], P(('grp', 'sp'), 'tp'), parts along dimension 0
- first_read: bfloat16 [8, 8, 128], P(('grp', 'sp'), 'tp'), parts along dimension 0
There are 2 independent parts, one for each index of `grp`. A program takes and returns all parts, laid end to end along the dimension named above; an argument that names none is the same for every part. Nothing has to cross between parts.
All inputs are finite; a program needn't handle non-finite values.
Results may differ from a plain program's by a relative error of at most 0.012.
Values may be sent and summed in bfloat16 or wider, within the bound.
A program may use at most 64 MiB of HBM per device.

v0:
```python
import jax
import jax.numpy as jnp
from jax import lax
from jax.sharding import PartitionSpec as P

HEADS = 8
DK = 128
CONV = 4
epsilon = 1e-06


def shifted(block, axis, distance):
    devices = range(lax.axis_size(axis))
    route = [(i - distance, i) for i in devices if i - distance in devices]
    return lax.ppermute(block, axis, route)


def project_rows(
    token_rows, norm_gain, key_weight, value_weight, input_gate_weight, forget_gate_weight
):
    widened = token_rows.astype(jnp.float32)
    normed = (
        widened
        * lax.rsqrt(jnp.mean(widened * widened, axis=-1, keepdims=True) + epsilon)
        * norm_gain.astype(jnp.float32)
    ).astype(jnp.bfloat16)
    key_matrix = key_weight.reshape(key_weight.shape[0], HEADS, DK)
    value_matrix = value_weight.reshape(value_weight.shape[0], HEADS, DK)
    key_linear = jnp.einsum(
        "apd,dhk->ahpk", normed, key_matrix, preferred_element_type=jnp.float32
    ).astype(jnp.bfloat16)
    values = jnp.einsum(
        "apd,dhk->ahpk", normed, value_matrix, preferred_element_type=jnp.float32
    ).astype(jnp.bfloat16)
    input_linear = jnp.einsum(
        "apd,dh->ahp", normed, input_gate_weight, preferred_element_type=jnp.float32
    ).astype(jnp.bfloat16)
    forget_linear = jnp.einsum(
        "apd,dh->ahp", normed, forget_gate_weight, preferred_element_type=jnp.float32
    ).astype(jnp.bfloat16)
    return (key_linear, values, input_linear, forget_linear)


def convolve(key_linear, previous, conv_weight):
    extended = jnp.concatenate([previous, key_linear], axis=2).astype(jnp.float32)
    length = key_linear.shape[2]
    tap_weight = conv_weight.reshape(CONV, HEADS, 1, DK)
    summed = extended[:, :, 0:length, :] * tap_weight[0]
    for offset in range(1, CONV):
        summed = summed + extended[:, :, offset : offset + length, :] * tap_weight[offset]
    return jax.nn.silu(summed).astype(jnp.bfloat16)


def read_cache(
    keys,
    values,
    input_linear,
    forget_linear,
    input_shift,
    forget_shift,
    new_query,
    new_key,
    new_value,
    new_input,
    new_forget,
):
    scaling = DK ** (-0.5)
    log_forget = jax.nn.log_sigmoid(forget_linear.astype(jnp.float32) + forget_shift)
    suffix = lax.cumsum(log_forget, axis=2, reverse=True) - log_forget
    new_decay = jax.nn.log_sigmoid(new_forget)
    log_weight = input_linear.astype(jnp.float32) + input_shift + suffix + new_decay[:, :, None]
    largest = jnp.maximum(jnp.max(log_weight, axis=2), new_input)
    weight_cache = jnp.exp(log_weight - largest[:, :, None])
    new_weight = jnp.exp(new_input - largest)
    matched = jnp.einsum("bhlk,bhk->bhl", keys, new_query, preferred_element_type=jnp.float32)
    scores = (weight_cache * matched * scaling).astype(jnp.bfloat16)
    fresh_match = jnp.sum(new_key.astype(jnp.float32) * new_query.astype(jnp.float32), axis=2)
    new_score = (new_weight * fresh_match * scaling).astype(jnp.bfloat16)
    denominator = jnp.sum(scores.astype(jnp.float32), axis=2) + new_score.astype(jnp.float32)
    numerator = jnp.einsum("bhl,bhlk->bhk", scores, values, preferred_element_type=jnp.float32)
    numerator = numerator + new_score.astype(jnp.float32)[:, :, None] * new_value.astype(
        jnp.float32
    )
    first_read = (numerator / jnp.maximum(jnp.abs(denominator), 1.0)[:, :, None]).astype(
        jnp.bfloat16
    )
    return (weight_cache, first_read)


def shards(
    layer_input,
    norm_gain,
    key_weight,
    value_weight,
    input_gate_weight,
    forget_gate_weight,
    conv_weight,
    input_shift,
    forget_shift,
    new_query,
    new_key,
    new_value,
    new_input,
    new_forget,
):
    key_linear, values, input_linear, forget_linear = project_rows(
        layer_input, norm_gain, key_weight, value_weight, input_gate_weight, forget_gate_weight
    )
    previous = shifted(key_linear[:, :, -(CONV - 1) :, :], "sp", 1)
    keys = convolve(key_linear, previous, conv_weight)
    keys, values, input_linear, forget_linear = (
        lax.all_to_all(
            lax.all_to_all(keys, "tp", split_axis=1, concat_axis=0, tiled=True),
            "sp",
            split_axis=0,
            concat_axis=2,
            tiled=True,
        ),
        lax.all_to_all(
            lax.all_to_all(values, "tp", split_axis=1, concat_axis=0, tiled=True),
            "sp",
            split_axis=0,
            concat_axis=2,
            tiled=True,
        ),
        lax.all_to_all(
            lax.all_to_all(input_linear, "tp", split_axis=1, concat_axis=0, tiled=True),
            "sp",
            split_axis=0,
            concat_axis=2,
            tiled=True,
        ),
        lax.all_to_all(
            lax.all_to_all(forget_linear, "tp", split_axis=1, concat_axis=0, tiled=True),
            "sp",
            split_axis=0,
            concat_axis=2,
            tiled=True,
        ),
    )
    weight_cache, first_read = read_cache(
        keys,
        values,
        input_linear,
        forget_linear,
        input_shift,
        forget_shift,
        new_query,
        new_key,
        new_value,
        new_input,
        new_forget,
    )
    return (keys, values, weight_cache, first_read)


def solution(mesh):
    in_specs = (
        P(("grp", "tp"), "sp", None),
        P(),
        P(),
        P(),
        P(),
        P(),
        P(),
        P(("grp", "sp"), "tp", None),
        P(("grp", "sp"), "tp", None),
        P(("grp", "sp"), "tp", None),
        P(("grp", "sp"), "tp", None),
        P(("grp", "sp"), "tp", None),
        P(("grp", "sp"), "tp"),
        P(("grp", "sp"), "tp"),
    )
    out_specs = (
        P(("grp", "sp"), "tp", None, None),
        P(("grp", "sp"), "tp", None, None),
        P(("grp", "sp"), "tp", None),
        P(("grp", "sp"), "tp", None),
    )
    return jax.shard_map(shards, mesh=mesh, in_specs=in_specs, out_specs=out_specs, check_vma=False)
```

profile of v0, /device:TPU:0, one launch (start us, length us, event | category | flops | bytes accessed | tf_op | source)
XLA Modules:
  0.0 106.6 jit_solution(14466072062410166473)
XLA Ops:
  1.4 1.5 %fusion.6 = f32[256]{0:T(256)S(1)} fusion(bf16[1,256,2048]{2,1,0:T(8,128)(2,1)} %param.14), kind=kLoop, calls=%fused_computation.8 | loop fusion | flops 1572608 | bytes 1049600 | tf_op jit(solution)/shard_map/reduce_sum | solution.py:24
  3.0 1.7 %fusion.22 = bf16[1,8,256]{2,1,0:T(8,128)(2,1)S(1)} fusion(bf16[2048,8]{0,1:T(8,128)(2,1)S(1)} %copy-done, bf16[1,256,2048]{2,1,0:T(8,128)(2,1)} %param.14, f32[2048]{0:T(1024)S(1)} %convert_element_type.131, f32[256]{0:T(256)S(1)} %add_rsqrt_fusion), kind=kOutput, calls=%fused_computation.18 | convolution fusion | flops 10487808 | bytes 1094656 | tf_op jit(solution)/shard_map/apd,dh->ahp/dot_general | solution.py:38
  6.5 6.3 %all-to-all-start.6 = ((bf16[4,2,256]{2,1,0:T(2,128)(2,1)}), bf16[4,2,256]{2,1,0:T(2,128)(2,1)S(1)}, u32[]{:S(2)}, u32[]{:S(2)}) async-start(bf16[4,2,256]{2,1,0:T(2,128)(2,1)} %reshape.225), calls=%async_computation.6 | async-start | bytes 8192 | tf_op jit(solution)/shard_map/all_to_all | solution.py:134
  14.6 3.8 %all-to-all-done.6 = bf16[4,2,256]{2,1,0:T(2,128)(2,1)S(1)} async-done(((bf16[4,2,256]{2,1,0:T(2,128)(2,1)}), bf16[4,2,256]{2,1,0:T(2,128)(2,1)S(1)}, u32[]{:S(2)}, u32[]{:S(2)}) %all-to-all-start.6) | async-done | bytes 4128 | tf_op jit(solution)/shard_map/all_to_all | solution.py:134
  18.4 3.2 %all-to-all-start.4 = ((bf16[4,2,256]{2,1,0:T(2,128)(2,1)}), bf16[4,2,256]{2,1,0:T(2,128)(2,1)S(1)}, u32[]{:S(2)}, u32[]{:S(2)}) async-start(bf16[4,2,256]{2,1,0:T(2,128)(2,1)} %reshape.227), calls=%async_computation.4 | async-start | bytes 8192 | tf_op jit(solution)/shard_map/all_to_all | solution.py:127
  22.3 4.9 %all-to-all-done.4 = bf16[4,2,256]{2,1,0:T(2,128)(2,1)S(1)} async-done(((bf16[4,2,256]{2,1,0:T(2,128)(2,1)}), bf16[4,2,256]{2,1,0:T(2,128)(2,1)S(1)}, u32[]{:S(2)}, u32[]{:S(2)}) %all-to-all-start.4) | async-done | bytes 4128 | tf_op jit(solution)/shard_map/all_to_all | solution.py:127
  27.2 3.2 %all-to-all-start.7 = ((bf16[4,2,256]{2,1,0:T(2,128)(2,1)}), bf16[4,2,256]{2,1,0:T(2,128)(2,1)S(1)}, u32[]{:S(2)}, u32[]{:S(2)}) async-start(bf16[4,2,256]{2,1,0:T(2,128)(2,1)} %all_to_all.92), calls=%async_computation.7 | async-start | bytes 8192 | tf_op jit(solution)/shard_map/all_to_all | solution.py:133
  31.1 3.1 %all-to-all-done.7 = bf16[4,2,256]{2,1,0:T(2,128)(2,1)S(1)} async-done(((bf16[4,2,256]{2,1,0:T(2,128)(2,1)}), bf16[4,2,256]{2,1,0:T(2,128)(2,1)S(1)}, u32[]{:S(2)}, u32[]{:S(2)}) %all-to-all-start.7) | async-done | bytes 4128 | tf_op jit(solution)/shard_map/all_to_all | solution.py:133
  34.2 3.2 %all-to-all-start.5 = ((bf16[4,2,256]{2,1,0:T(2,128)(2,1)}), bf16[4,2,256]{2,1,0:T(2,128)(2,1)S(1)}, u32[]{:S(2)}, u32[]{:S(2)}) async-start(bf16[4,2,256]{2,1,0:T(2,128)(2,1)} %all_to_all.89), calls=%async_computation.5 | async-start | bytes 8192 | tf_op jit(solution)/shard_map/all_to_all | solution.py:126
  37.5 4.3 %fusion.15 = bf16[1,8,256,128]{3,2,0,1:T(8,128)(2,1)} fusion(bf16[1,256,2048]{2,1,0:T(8,128)(2,1)S(1)} %copy-done.3, f32[2048]{0:T(1024)S(1)} %convert_element_type.131, f32[256]{0:T(256)S(1)} %add_rsqrt_fusion, bf16[2048,1024]{1,0:T(8,128)(2,1)} %param.17), kind=kOutput, calls=%fused_computation.13 | convolution fusion | flops 1076101120 | bytes 5776384 | tf_op jit(solution)/shard_map/apd,dhk->ahpk/dot_general | solution.py:32
  41.8 4.1 %all-to-all-start.2 = ((bf16[1,8,256,128]{3,2,0,1:T(8,128)(2,1)}), bf16[1,8,256,128]{3,2,0,1:T(8,128)(2,1)}, u32[]{:S(2)}, u32[]{:S(2)}) async-start(bf16[1,8,256,128]{3,2,0,1:T(8,128)(2,1)} %fusion.15), calls=%async_computation.2 | async-start | bytes 1048576 | tf_op jit(solution)/shard_map/all_to_all | solution.py:120
  45.9 3.5 %fusion.18 = bf16[1,8,256,128]{3,2,1,0:T(8,128)(2,1)S(1)} fusion(bf16[1,256,2048]{2,1,0:T(8,128)(2,1)S(1)} %copy-done.3, f32[2048]{0:T(1024)S(1)} %convert_element_type.131, f32[256]{0:T(256)S(1)} %add_rsqrt_fusion, bf16[2048,1024]{1,0:T(8,128)(2,1)} %param.16), kind=kOutput, calls=%fused_computation.14 | convolution fusion | flops 1076101120 | bytes 5776384 | tf_op jit(solution)/shard_map/apd,dhk->ahpk/dot_general | solution.py:29
  49.4 2.4 %collective-permute-start = (bf16[1,8,3,128]{3,2,1,0:T(4,128)(2,1)S(1)}, bf16[1,8,3,128]{3,2,1,0:T(4,128)(2,1)S(1)}, u32[]{:S(2)}, u32[]{:S(2)}) collective-permute-start(bf16[1,8,3,128]{3,2,1,0:T(4,128)(2,1)S(1)} %slice.48), channel_id=1, source_target_pairs={{0,4},{4,8},{8,12},{1,5},{5,9},{9,13},{2,6},{6,10},{10,14},{3,7},{... | collective-permute-start | bytes 18440 | tf_op jit(solution)/shard_map/ppermute | solution.py:15
  51.8 0.8 collective-permute-done
  52.8 1.5 %fusion.30 = bf16[1,8,256,128]{3,2,0,1:T(8,128)(2,1)} fusion(f32[8,128]{1,0:T(8,128)S(1)} %bitcast.172, f32[1,8,259,128]{3,2,1,0:T(8,128)S(1)} %maximum_convert_fusion, f32[8,128]{1,0:T(8,128)S(1)} %bitcast.173, f32[8,128]{1,0:T(8,128)S(1)} %bitcast.171, f32[8,128]{1,0:T(8,128)S(1)} %bitcast.170), kind=kLoop, calls=%fused_computation.32 | loop fusion | flops 3145728 | bytes 4734976 | tf_op jit(solution)/shard_map/convert_element_type | solution.py:51
  54.2 7.1 %all-to-all-done.2 = bf16[1,8,256,128]{3,2,0,1:T(8,128)(2,1)} async-done(((bf16[1,8,256,128]{3,2,0,1:T(8,128)(2,1)}), bf16[1,8,256,128]{3,2,0,1:T(8,128)(2,1)}, u32[]{:S(2)}, u32[]{:S(2)}) %all-to-all-start.2) | async-done | bytes 524320 | tf_op jit(solution)/shard_map/all_to_all | solution.py:120
  61.4 4.1 %all-to-all-start = ((bf16[1,8,256,128]{3,2,0,1:T(8,128)(2,1)}), bf16[1,8,256,128]{3,2,0,1:T(8,128)(2,1)}, u32[]{:S(2)}, u32[]{:S(2)}) async-start(bf16[1,8,256,128]{3,2,0,1:T(8,128)(2,1)} %fusion.30), calls=%async_computation | async-start | bytes 1048576 | tf_op jit(solution)/shard_map/all_to_all | solution.py:113
  65.7 2.5 %reduce-window.6 = f32[1,2,8,128]{3,2,1,0:T(8,128)S(1)} reduce-window(f32[1,2,8,128]{3,2,1,0:T(8,128)S(1)} %copy.82, f32[]{:T(128)} %constant.7.clone.1), window={size=1x1x1x128 pad=0_0x0_0x0_0x0_127}, to_apply=%region_1.2 | reduce-window | flops 260096 | bytes 16388 | tf_op jit(solution)/shard_map/reduce-window
  68.5 11.6 %all-to-all-done = bf16[1,8,256,128]{3,2,0,1:T(8,128)(2,1)} async-done(((bf16[1,8,256,128]{3,2,0,1:T(8,128)(2,1)}), bf16[1,8,256,128]{3,2,0,1:T(8,128)(2,1)}, u32[]{:S(2)}, u32[]{:S(2)}) %all-to-all-start) | async-done | bytes 524320 | tf_op jit(solution)/shard_map/all_to_all | solution.py:113
  80.1 3.5 %all-to-all-start.3 = ((bf16[4,2,256,128]{3,2,1,0:T(8,128)(2,1)}), bf16[4,2,256,128]{3,2,1,0:T(8,128)(2,1)S(1)}, u32[]{:S(2)}, u32[]{:S(2)}) async-start(bf16[4,2,256,128]{3,2,1,0:T(8,128)(2,1)} %bitcast.18), calls=%async_computation.3 | async-start | bytes 1048576 | tf_op jit(solution)/shard_map/all_to_all | solution.py:119
  83.7 8.6 %all-to-all-done.3 = bf16[4,2,256,128]{3,2,1,0:T(8,128)(2,1)S(1)} async-done(((bf16[4,2,256,128]{3,2,1,0:T(8,128)(2,1)}), bf16[4,2,256,128]{3,2,1,0:T(8,128)(2,1)S(1)}, u32[]{:S(2)}, u32[]{:S(2)}) %all-to-all-start.3) | async-done | bytes 524320 | tf_op jit(solution)/shard_map/all_to_all | solution.py:119
  92.3 3.6 %all-to-all-start.1 = ((bf16[4,2,256,128]{3,2,1,0:T(8,128)(2,1)}), bf16[4,2,256,128]{3,2,1,0:T(8,128)(2,1)S(1)}, u32[]{:S(2)}, u32[]{:S(2)}) async-start(bf16[4,2,256,128]{3,2,1,0:T(8,128)(2,1)} %bitcast.10), calls=%async_computation.1 | async-start | bytes 1048576 | tf_op jit(solution)/shard_map/all_to_all | solution.py:112
  96.2 8.5 %all-to-all-done.1 = bf16[4,2,256,128]{3,2,1,0:T(8,128)(2,1)S(1)} async-done(((bf16[4,2,256,128]{3,2,1,0:T(8,128)(2,1)}), bf16[4,2,256,128]{3,2,1,0:T(8,128)(2,1)S(1)}, u32[]{:S(2)}, u32[]{:S(2)}) %all-to-all-start.1) | async-done | bytes 524320 | tf_op jit(solution)/shard_map/all_to_all | solution.py:112
  105.0 0.8 convert_reduce_fusion
  (66 shorter events, 7.7 us)
Async XLA Ops:
  0.6 2.3 %copy-start = (bf16[2048,8]{0,1:T(8,128)(2,1)S(1)}, bf16[2048,8]{0,1:T(8,128)(2,1)}, u32[]{:S(2)}) copy-start(bf16[2048,8]{0,1:T(8,128)(2,1)} %param.19) | copy-start | bytes 98308
  0.6 12.2 %copy-start.3 = (bf16[1,256,2048]{2,1,0:T(8,128)(2,1)S(1)}, bf16[1,256,2048]{2,1,0:T(8,128)(2,1)}, u32[]{:S(2)}) copy-start(bf16[1,256,2048]{2,1,0:T(8,128)(2,1)} %param.14) | copy-start | bytes 3145732
  0.7 12.2 %copy-start.10 = (bf16[2048,8]{0,1:T(8,128)(2,1)S(1)}, bf16[2048,8]{0,1:T(8,128)(2,1)}, u32[]{:S(2)}) copy-start(bf16[2048,8]{0,1:T(8,128)(2,1)} %param.18) | copy-start | bytes 98308
  6.5 11.9 %all-to-all-start.6 = ((bf16[4,2,256]{2,1,0:T(2,128)(2,1)}), bf16[4,2,256]{2,1,0:T(2,128)(2,1)S(1)}, u32[]{:S(2)}, u32[]{:S(2)}) async-start(bf16[4,2,256]{2,1,0:T(2,128)(2,1)} %reshape.225), calls=%async_computation.6 | async-start | bytes 8192 | tf_op jit(solution)/shard_map/all_to_all | solution.py:134
  18.4 8.8 %all-to-all-start.4 = ((bf16[4,2,256]{2,1,0:T(2,128)(2,1)}), bf16[4,2,256]{2,1,0:T(2,128)(2,1)S(1)}, u32[]{:S(2)}, u32[]{:S(2)}) async-start(bf16[4,2,256]{2,1,0:T(2,128)(2,1)} %reshape.227), calls=%async_computation.4 | async-start | bytes 8192 | tf_op jit(solution)/shard_map/all_to_all | solution.py:127
  27.2 7.0 %all-to-all-start.7 = ((bf16[4,2,256]{2,1,0:T(2,128)(2,1)}), bf16[4,2,256]{2,1,0:T(2,128)(2,1)S(1)}, u32[]{:S(2)}, u32[]{:S(2)}) async-start(bf16[4,2,256]{2,1,0:T(2,128)(2,1)} %all_to_all.92), calls=%async_computation.7 | async-start | bytes 8192 | tf_op jit(solution)/shard_map/all_to_all | solution.py:133
  34.2 7.5 %all-to-all-start.5 = ((bf16[4,2,256]{2,1,0:T(2,128)(2,1)}), bf16[4,2,256]{2,1,0:T(2,128)(2,1)S(1)}, u32[]{:S(2)}, u32[]{:S(2)}) async-start(bf16[4,2,256]{2,1,0:T(2,128)(2,1)} %all_to_all.89), calls=%async_computation.5 | async-start | bytes 8192 | tf_op jit(solution)/shard_map/all_to_all | solution.py:126
  41.8 19.6 %all-to-all-start.2 = ((bf16[1,8,256,128]{3,2,0,1:T(8,128)(2,1)}), bf16[1,8,256,128]{3,2,0,1:T(8,128)(2,1)}, u32[]{:S(2)}, u32[]{:S(2)}) async-start(bf16[1,8,256,128]{3,2,0,1:T(8,128)(2,1)} %fusion.15), calls=%async_computation.2 | async-start | bytes 1048576 | tf_op jit(solution)/shard_map/all_to_all | solution.py:120
  45.9 5.9 %copy-start.5 = (f32[4,1024]{1,0:T(4,128)S(1)}, f32[4,1024]{1,0:T(4,128)}, u32[]{:S(2)}) copy-start(f32[4,1024]{1,0:T(4,128)} %param.20) | copy-start | bytes 49156
  49.4 3.2 %collective-permute-start = (bf16[1,8,3,128]{3,2,1,0:T(4,128)(2,1)S(1)}, bf16[1,8,3,128]{3,2,1,0:T(4,128)(2,1)S(1)}, u32[]{:S(2)}, u32[]{:S(2)}) collective-permute-start(bf16[1,8,3,128]{3,2,1,0:T(4,128)(2,1)S(1)} %slice.48), channel_id=1, source_target_pairs={{0,4},{4,8},{8,12},{1,5},{5,9},{9,13},{2,6},{6,10},{10,14},{3,7},{... | collective-permute-start | bytes 18440 | tf_op jit(solution)/shard_map/ppermute | solution.py:15
  52.7 12.8 %copy-start.7 = (bf16[1,2,128]{2,1,0:T(2,128)(2,1)S(1)}, bf16[1,2,128]{2,1,0:T(2,128)(2,1)}, u32[]{:S(2)}) copy-start(bf16[1,2,128]{2,1,0:T(2,128)(2,1)} %param.23) | copy-start | bytes 1540
  52.7 12.8 %copy-start.11 = (bf16[1,2,128]{2,1,0:T(2,128)(2,1)S(1)}, bf16[1,2,128]{2,1,0:T(2,128)(2,1)}, u32[]{:S(2)}) copy-start(bf16[1,2,128]{2,1,0:T(2,128)(2,1)} %param.24) | copy-start | bytes 1540
  52.8 12.9 %copy-start.12 = (f32[1,2]{1,0:T(1,128)S(1)}, f32[1,2]{1,0:T(1,128)}, u32[]{:S(2)}) copy-start(f32[1,2]{1,0:T(1,128)} %param.27) | copy-start | bytes 28
  52.8 12.9 %copy-start.4 = (f32[1,2,1024]{2,1,0:T(2,128)S(1)}, f32[1,2,1024]{2,1,0:T(2,128)}, u32[]{:S(2)}) copy-start(f32[1,2,1024]{2,1,0:T(2,128)} %param.22) | copy-start | bytes 24580
  54.2 41.7 %copy-start.6 = (f32[1,2,1024]{2,1,0:T(2,128)S(1)}, f32[1,2,1024]{2,1,0:T(2,128)}, u32[]{:S(2)}) copy-start(f32[1,2,1024]{2,1,0:T(2,128)} %param.21) | copy-start | bytes 24580
  54.2 41.9 %copy-start.8 = (f32[1,2]{1,0:T(1,128)S(1)}, f32[1,2]{1,0:T(1,128)}, u32[]{:S(2)}) copy-start(f32[1,2]{1,0:T(1,128)} %param.26) | copy-start | bytes 28
  61.4 18.7 %all-to-all-start = ((bf16[1,8,256,128]{3,2,0,1:T(8,128)(2,1)}), bf16[1,8,256,128]{3,2,0,1:T(8,128)(2,1)}, u32[]{:S(2)}, u32[]{:S(2)}) async-start(bf16[1,8,256,128]{3,2,0,1:T(8,128)(2,1)} %fusion.30), calls=%async_computation | async-start | bytes 1048576 | tf_op jit(solution)/shard_map/all_to_all | solution.py:113
  80.1 12.3 %all-to-all-start.3 = ((bf16[4,2,256,128]{3,2,1,0:T(8,128)(2,1)}), bf16[4,2,256,128]{3,2,1,0:T(8,128)(2,1)S(1)}, u32[]{:S(2)}, u32[]{:S(2)}) async-start(bf16[4,2,256,128]{3,2,1,0:T(8,128)(2,1)} %bitcast.18), calls=%async_computation.3 | async-start | bytes 1048576 | tf_op jit(solution)/shard_map/all_to_all | solution.py:119
  92.3 13.7 %copy-start.9 = (bf16[1,2,128]{2,1,0:T(2,128)(2,1)S(1)}, bf16[1,2,128]{2,1,0:T(2,128)(2,1)}, u32[]{:S(2)}) copy-start(bf16[1,2,128]{2,1,0:T(2,128)(2,1)} %param.25) | copy-start | bytes 1540
  92.3 12.4 %all-to-all-start.1 = ((bf16[4,2,256,128]{3,2,1,0:T(8,128)(2,1)}), bf16[4,2,256,128]{3,2,1,0:T(8,128)(2,1)S(1)}, u32[]{:S(2)}, u32[]{:S(2)}) async-start(bf16[4,2,256,128]{3,2,1,0:T(8,128)(2,1)} %bitcast.10), calls=%async_computation.1 | async-start | bytes 1048576 | tf_op jit(solution)/shard_map/all_to_all | solution.py:112
  96.2 10.4 %copy-start.1 = (bf16[4,2,256,128]{3,2,0,1:T(8,128)(2,1)}, bf16[4,2,256,128]{3,2,0,1:T(8,128)(2,1)S(1)}, u32[]{:S(2)}) copy-start(bf16[4,2,256,128]{3,2,0,1:T(8,128)(2,1)S(1)} %copy.45) | copy-start | bytes 1572868
  104.8 1.9 %copy-start.2 = (bf16[4,2,256,128]{3,2,0,1:T(8,128)(2,1)}, bf16[4,2,256,128]{3,2,0,1:T(8,128)(2,1)S(1)}, u32[]{:S(2)}) copy-start(bf16[4,2,256,128]{3,2,0,1:T(8,128)(2,1)S(1)} %copy.42) | copy-start | bytes 1572868
where the time goes:
time: 107 us
  waiting for transfers between devices  48.4 us (45%)
  starting transfers between devices  33.8 us (32%)
  matrix products  10.3 us (10%)
  other arithmetic  9.68 us (9%)
  local copies, waits for them, and re-layouts  3.49 us (3%)
    all_to_all x1, waiting for transfers between devices, shards(): lax.all_to_all(keys, 'tp', split_axis=1, concat_axis=0, tiled=True)  11.6 us
    all_to_all x1, waiting for transfers between devices, shards(): lax.all_to_all(lax.all_to_all(values, 'tp', split_axis=1, concat_axis=0,...  8.61 us
    all_to_all x1, waiting for transfers between devices, shards(): lax.all_to_all(lax.all_to_all(keys, 'tp', split_axis=1, concat_axis=0, ti...  8.51 us
    all_to_all x1, waiting for transfers between devices, shards(): lax.all_to_all(values, 'tp', split_axis=1, concat_axis=0, tiled=True)  7.12 us
    all_to_all x1, starting transfers between devices, shards(): lax.all_to_all(forget_linear, 'tp', split_axis=1, concat_axis=0, tiled=True)  6.35 us
    all_to_all x1, waiting for transfers between devices, shards(): lax.all_to_all(input_linear, 'tp', split_axis=1, concat_axis=0, tiled=True)  4.89 us
    dot_general x1, matrix products, project_rows(): jnp.einsum('apd,dhk->ahpk', normed, value_matrix, preferred_element_type=...  4.29 us
    all_to_all x1, starting transfers between devices, shards(): lax.all_to_all(values, 'tp', split_axis=1, concat_axis=0, tiled=True)  4.14 us
  transfers between devices with their start and end apart: 9, of which 8 were waited for; matrix products, arithmetic and copies ran while one was open for 14% of the time, Pallas kernels for 0%

commit v1 on v0

--- a/solution.py
+++ b/solution.py
@@ -7,6 +7,28 @@
 DK = 128
 CONV = 4
 epsilon = 1e-06
+
+
+def split_up(x, dim, size):
+    before, after = (x.shape[:dim], x.shape[dim + 1 :])
+    return jnp.moveaxis(x.reshape(*before, size, -1, *after), dim, 0)
+
+
+def laid_out(tiles, dim):
+    shape = list(tiles.shape[1:])
+    shape[dim] *= tiles.shape[0]
+    return jnp.moveaxis(tiles, 0, dim).reshape(shape)
+
+
+def rotated_exchange(shard, axis, split_dim, concat_dim):
+    size, index = (lax.axis_size(axis), lax.axis_index(axis))
+    pieces = split_up(shard, split_dim, size)
+    gathered = [pieces[index]]
+    for lap in range(1, size):
+        sent = pieces[(index + lap) % size]
+        gathered.append(lax.ppermute(sent, axis, [(i, (i + lap) % size) for i in range(size)]))
+    pieces = jnp.stack(gathered)[(index - jnp.arange(size)) % size]
+    return laid_out(pieces, concat_dim)
 
 
 def shifted(block, axis, distance):
@@ -131,7 +153,7 @@
             tiled=True,
         ),
         lax.all_to_all(
-            lax.all_to_all(forget_linear, "tp", split_axis=1, concat_axis=0, tiled=True),
+            rotated_exchange(forget_linear, "tp", 1, 0),
             "sp",
             split_axis=0,
             concat_axis=2,

time: 107 us -> 103 us (0.963)
  waiting for transfers between devices: 48.4 us -> 44 us
    all_to_all x2 -> x1, starting transfers between devices: 9.59 us -> 3.25 us  [shards(): lax.all_to_all(rotated_exchange(forget_linear, 'tp', 1, 0), 'sp', split_a...]
    ppermute x0 -> x3, starting transfers between devices: none -> 6.14 us  [rotated_exchange(): lax.ppermute(sent, axis, [(i, (i + lap) % size) for i in range(size)])]
    all_to_all x2 -> x1, waiting for transfers between devices: 6.92 us -> 3.1 us  [shards(): lax.all_to_all(rotated_exchange(forget_linear, 'tp', 1, 0), 'sp', split_a...]
    gather x0 -> x1, local copies, waits for them, and re-layouts: none -> 1.16 us  [rotated_exchange(): pieces = jnp.stack(gathered)[(index - jnp.arange(size)) % size]]
    another operation x2 -> x3, other arithmetic: 2.68 us -> 2.7 us
  transfers between devices with their start and end apart: 9 -> 11, of which waited for: 8 -> 7; matrix products, arithmetic and copies ran while one was open for 14% -> 16% of each run, Pallas kernels for 0% -> 0%
where the time goes in v1:
time: 103 us; the launch traced here: 102 us
  waiting for transfers between devices  44 us (43%)
  starting transfers between devices  34.4 us (33%)
  matrix products  10.3 us (10%)
  other arithmetic  9.03 us (9%)
  local copies, waits for them, and re-layouts  3.4 us (3%)
  between operations  1.03 us (1%)
    all_to_all x1, waiting for transfers between devices, shards(): lax.all_to_all(keys, 'tp', split_axis=1, concat_axis=0, tiled=True)  11.6 us
    all_to_all x1, waiting for transfers between devices, shards(): lax.all_to_all(lax.all_to_all(values, 'tp', split_axis=1, concat_axis=0,...  8.61 us
    all_to_all x1, waiting for transfers between devices, shards(): lax.all_to_all(lax.all_to_all(keys, 'tp', split_axis=1, concat_axis=0, ti...  8.51 us
    all_to_all x1, waiting for transfers between devices, shards(): lax.all_to_all(values, 'tp', split_axis=1, concat_axis=0, tiled=True)  7.11 us
    ppermute x3, starting transfers between devices, rotated_exchange(): lax.ppermute(sent, axis, [(i, (i + lap) % size) for i in range(size)])  6.14 us
    all_to_all x1, waiting for transfers between devices, shards(): lax.all_to_all(input_linear, 'tp', split_axis=1, concat_axis=0, tiled=True)  4.34 us
    dot_general x1, matrix products, project_rows(): jnp.einsum('apd,dhk->ahpk', normed, value_matrix, preferred_element_type=...  4.29 us
    all_to_all x1, starting transfers between devices, shards(): lax.all_to_all(keys, 'tp', split_axis=1, concat_axis=0, tiled=True)  4.14 us
  transfers between devices with their start and end apart: 11, of which 7 were waited for; matrix products, arithmetic and copies ran while one was open for 16% of the time, Pallas kernels for 0%

profile of v1, /device:TPU:0, one launch (start us, length us, event | category | flops | bytes accessed | tf_op | source)
XLA Modules:
  0.0 102.2 jit_solution(8638553539271028213)
XLA Ops:
  1.5 1.5 %fusion.6 = f32[256]{0:T(256)S(1)} fusion(bf16[1,256,2048]{2,1,0:T(8,128)(2,1)} %param.14), kind=kLoop, calls=%fused_computation.9 | loop fusion | flops 1572608 | bytes 1049600 | tf_op jit(solution)/shard_map/reduce_sum | solution.py:46
  3.0 1.7 %fusion.22 = bf16[8,256]{1,0:T(8,128)(2,1)S(1)} fusion(bf16[2048,8]{0,1:T(8,128)(2,1)S(1)} %copy-done, bf16[1,256,2048]{2,1,0:T(8,128)(2,1)} %param.14, f32[2048]{0:T(1024)S(1)} %convert_element_type.129, f32[256]{0:T(256)S(1)} %add_rsqrt_fusion), kind=kOutput, calls=%fused_computation.19 | convolution fusion | flops 10487808 | bytes 1094656 | tf_op jit(solution)/shard_map/apd,dh->ahp/dot_general | solution.py:60
  4.7 5.1 %collective-permute-start.3 = (bf16[1,2,256]{2,1,0:T(2,128)(2,1)S(1)}, bf16[1,2,256]{2,1,0:T(2,128)(2,1)S(1)}, u32[]{:S(2)}, u32[]{:S(2)}) collective-permute-start(bf16[1,2,256]{2,1,0:T(2,128)(2,1)S(1)} %get-tuple-element.16), channel_id=1, source_target_pairs={{0,3},{1,0},{2,1},{3,2},{4,7},{5,4},{6,5},{7,6},{8,11},{9,8},{10,9... | collective-permute-start | bytes 3080 | tf_op jit(solution)/shard_map/ppermute | solution.py:29
  9.8 1.0 collective-permute-start.1
  13.1 4.1 %all-to-all-start.4 = ((bf16[4,2,256]{2,1,0:T(2,128)(2,1)}), bf16[4,2,256]{2,1,0:T(2,128)(2,1)S(1)}, u32[]{:S(2)}, u32[]{:S(2)}) async-start(bf16[4,2,256]{2,1,0:T(2,128)(2,1)} %reshape.286), calls=%async_computation.4 | async-start | bytes 8192 | tf_op jit(solution)/shard_map/all_to_all | solution.py:149
  17.3 1.2 %gather_fusion = bf16[4,2,256]{2,1,0:T(2,128)(2,1)} fusion(bf16[4,2,256]{2,1,0:T(2,128)(2,1)S(1)} %maximum_bitcast_fusion, s32[1024]{0:T(1024)S(1)} %pad_clamp_fusion), kind=kCustom, calls=%fused_computation | custom fusion | bytes 8208 | tf_op jit(solution)/shard_map/gather | solution.py:30
  18.5 4.3 %all-to-all-done.4 = bf16[4,2,256]{2,1,0:T(2,128)(2,1)S(1)} async-done(((bf16[4,2,256]{2,1,0:T(2,128)(2,1)}), bf16[4,2,256]{2,1,0:T(2,128)(2,1)S(1)}, u32[]{:S(2)}, u32[]{:S(2)}) %all-to-all-start.4) | async-done | bytes 4128 | tf_op jit(solution)/shard_map/all_to_all | solution.py:149
  22.8 3.2 %all-to-all-start.6 = ((bf16[4,2,256]{2,1,0:T(2,128)(2,1)}), bf16[4,2,256]{2,1,0:T(2,128)(2,1)S(1)}, u32[]{:S(2)}, u32[]{:S(2)}) async-start(bf16[4,2,256]{2,1,0:T(2,128)(2,1)} %gather_fusion), calls=%async_computation.6 | async-start | bytes 8192 | tf_op jit(solution)/shard_map/all_to_all | solution.py:155
  26.7 3.1 %all-to-all-done.6 = bf16[4,2,256]{2,1,0:T(2,128)(2,1)S(1)} async-done(((bf16[4,2,256]{2,1,0:T(2,128)(2,1)}), bf16[4,2,256]{2,1,0:T(2,128)(2,1)S(1)}, u32[]{:S(2)}, u32[]{:S(2)}) %all-to-all-start.6) | async-done | bytes 4128 | tf_op jit(solution)/shard_map/all_to_all | solution.py:155
  29.8 3.2 %all-to-all-start.5 = ((bf16[4,2,256]{2,1,0:T(2,128)(2,1)}), bf16[4,2,256]{2,1,0:T(2,128)(2,1)S(1)}, u32[]{:S(2)}, u32[]{:S(2)}) async-start(bf16[4,2,256]{2,1,0:T(2,128)(2,1)} %all_to_all.80), calls=%async_computation.5 | async-start | bytes 8192 | tf_op jit(solution)/shard_map/all_to_all | solution.py:148
  33.1 4.3 %fusion.15 = bf16[1,8,256,128]{3,2,0,1:T(8,128)(2,1)} fusion(bf16[1,256,2048]{2,1,0:T(8,128)(2,1)S(1)} %copy-done.3, f32[2048]{0:T(1024)S(1)} %convert_element_type.129, f32[256]{0:T(256)S(1)} %add_rsqrt_fusion, bf16[2048,1024]{1,0:T(8,128)(2,1)} %param.17), kind=kOutput, calls=%fused_computation.14 | convolution fusion | flops 1076101120 | bytes 5776384 | tf_op jit(solution)/shard_map/apd,dhk->ahpk/dot_general | solution.py:54
  37.4 4.1 %all-to-all-start.2 = ((bf16[1,8,256,128]{3,2,0,1:T(8,128)(2,1)}), bf16[1,8,256,128]{3,2,0,1:T(8,128)(2,1)}, u32[]{:S(2)}, u32[]{:S(2)}) async-start(bf16[1,8,256,128]{3,2,0,1:T(8,128)(2,1)} %fusion.15), calls=%async_computation.2 | async-start | bytes 1048576 | tf_op jit(solution)/shard_map/all_to_all | solution.py:142
  41.5 3.5 %fusion.18 = bf16[1,8,256,128]{3,2,1,0:T(8,128)(2,1)S(1)} fusion(bf16[1,256,2048]{2,1,0:T(8,128)(2,1)S(1)} %copy-done.3, f32[2048]{0:T(1024)S(1)} %convert_element_type.129, f32[256]{0:T(256)S(1)} %add_rsqrt_fusion, bf16[2048,1024]{1,0:T(8,128)(2,1)} %param.16), kind=kOutput, calls=%fused_computation.15 | convolution fusion | flops 1076101120 | bytes 5776384 | tf_op jit(solution)/shard_map/apd,dhk->ahpk/dot_general | solution.py:51
  45.0 2.3 %collective-permute-start = (bf16[1,8,3,128]{3,2,1,0:T(4,128)(2,1)S(1)}, bf16[1,8,3,128]{3,2,1,0:T(4,128)(2,1)S(1)}, u32[]{:S(2)}, u32[]{:S(2)}) collective-permute-start(bf16[1,8,3,128]{3,2,1,0:T(4,128)(2,1)S(1)} %slice.50), channel_id=1, source_target_pairs={{0,4},{4,8},{8,12},{1,5},{5,9},{9,13},{2,6},{6,10},{10,14},{3,7},{... | collective-permute-start | bytes 18440 | tf_op jit(solution)/shard_map/ppermute | solution.py:37
  48.4 1.5 %fusion.30 = bf16[1,8,256,128]{3,2,0,1:T(8,128)(2,1)} fusion(f32[8,128]{1,0:T(8,128)S(1)} %bitcast.177, f32[1,8,259,128]{3,2,1,0:T(8,128)S(1)} %maximum_convert_fusion, f32[8,128]{1,0:T(8,128)S(1)} %bitcast.178, f32[8,128]{1,0:T(8,128)S(1)} %bitcast.176, f32[8,128]{1,0:T(8,128)S(1)} %bitcast.175), kind=kLoop, calls=%fused_computation.33 | loop fusion | flops 3145728 | bytes 4734976 | tf_op jit(solution)/shard_map/convert_element_type | solution.py:73
  49.8 7.1 %all-to-all-done.2 = bf16[1,8,256,128]{3,2,0,1:T(8,128)(2,1)} async-done(((bf16[1,8,256,128]{3,2,0,1:T(8,128)(2,1)}), bf16[1,8,256,128]{3,2,0,1:T(8,128)(2,1)}, u32[]{:S(2)}, u32[]{:S(2)}) %all-to-all-start.2) | async-done | bytes 524320 | tf_op jit(solution)/shard_map/all_to_all | solution.py:142
  56.9 4.1 %all-to-all-start = ((bf16[1,8,256,128]{3,2,0,1:T(8,128)(2,1)}), bf16[1,8,256,128]{3,2,0,1:T(8,128)(2,1)}, u32[]{:S(2)}, u32[]{:S(2)}) async-start(bf16[1,8,256,128]{3,2,0,1:T(8,128)(2,1)} %fusion.30), calls=%async_computation | async-start | bytes 1048576 | tf_op jit(solution)/shard_map/all_to_all | solution.py:135
  61.3 2.5 %reduce-window.6 = f32[1,2,8,128]{3,2,1,0:T(8,128)S(1)} reduce-window(f32[1,2,8,128]{3,2,1,0:T(8,128)S(1)} %copy.79, f32[]{:T(128)} %constant.53.clone.1), window={size=1x1x1x128 pad=0_0x0_0x0_0x0_127}, to_apply=%region_1.2 | reduce-window | flops 260096 | bytes 16388 | tf_op jit(solution)/shard_map/reduce-window
  64.1 11.6 %all-to-all-done = bf16[1,8,256,128]{3,2,0,1:T(8,128)(2,1)} async-done(((bf16[1,8,256,128]{3,2,0,1:T(8,128)(2,1)}), bf16[1,8,256,128]{3,2,0,1:T(8,128)(2,1)}, u32[]{:S(2)}, u32[]{:S(2)}) %all-to-all-start) | async-done | bytes 524320 | tf_op jit(solution)/shard_map/all_to_all | solution.py:135
  75.7 3.5 %all-to-all-start.3 = ((bf16[4,2,256,128]{3,2,1,0:T(8,128)(2,1)}), bf16[4,2,256,128]{3,2,1,0:T(8,128)(2,1)S(1)}, u32[]{:S(2)}, u32[]{:S(2)}) async-start(bf16[4,2,256,128]{3,2,1,0:T(8,128)(2,1)} %bitcast.18), calls=%async_computation.3 | async-start | bytes 1048576 | tf_op jit(solution)/shard_map/all_to_all | solution.py:141
  79.3 8.6 %all-to-all-done.3 = bf16[4,2,256,128]{3,2,1,0:T(8,128)(2,1)S(1)} async-done(((bf16[4,2,256,128]{3,2,1,0:T(8,128)(2,1)}), bf16[4,2,256,128]{3,2,1,0:T(8,128)(2,1)S(1)}, u32[]{:S(2)}, u32[]{:S(2)}) %all-to-all-start.3) | async-done | bytes 524320 | tf_op jit(solution)/shard_map/all_to_all | solution.py:141
  87.9 3.6 %all-to-all-start.1 = ((bf16[4,2,256,128]{3,2,1,0:T(8,128)(2,1)}), bf16[4,2,256,128]{3,2,1,0:T(8,128)(2,1)S(1)}, u32[]{:S(2)}, u32[]{:S(2)}) async-start(bf16[4,2,256,128]{3,2,1,0:T(8,128)(2,1)} %bitcast.10), calls=%async_computation.1 | async-start | bytes 1048576 | tf_op jit(solution)/shard_map/all_to_all | solution.py:134
  91.8 8.5 %all-to-all-done.1 = bf16[4,2,256,128]{3,2,1,0:T(8,128)(2,1)S(1)} async-done(((bf16[4,2,256,128]{3,2,1,0:T(8,128)(2,1)}), bf16[4,2,256,128]{3,2,1,0:T(8,128)(2,1)S(1)}, u32[]{:S(2)}, u32[]{:S(2)}) %all-to-all-start.1) | async-done | bytes 524320 | tf_op jit(solution)/shard_map/all_to_all | solution.py:134
  100.6 0.8 convert_reduce_fusion
  (70 shorter events, 6.6 us)
Async XLA Ops:
  0.6 2.4 %copy-start = (bf16[2048,8]{0,1:T(8,128)(2,1)S(1)}, bf16[2048,8]{0,1:T(8,128)(2,1)}, u32[]{:S(2)}) copy-start(bf16[2048,8]{0,1:T(8,128)(2,1)} %param.19) | copy-start | bytes 98308
  0.6 10.2 %copy-start.3 = (bf16[1,256,2048]{2,1,0:T(8,128)(2,1)S(1)}, bf16[1,256,2048]{2,1,0:T(8,128)(2,1)}, u32[]{:S(2)}) copy-start(bf16[1,256,2048]{2,1,0:T(8,128)(2,1)} %param.14) | copy-start | bytes 3145732
  0.7 10.2 %copy-start.10 = (bf16[2048,8]{0,1:T(8,128)(2,1)S(1)}, bf16[2048,8]{0,1:T(8,128)(2,1)}, u32[]{:S(2)}) copy-start(bf16[2048,8]{0,1:T(8,128)(2,1)} %param.18) | copy-start | bytes 98308
  4.7 12.5 %collective-permute-start.3 = (bf16[1,2,256]{2,1,0:T(2,128)(2,1)S(1)}, bf16[1,2,256]{2,1,0:T(2,128)(2,1)S(1)}, u32[]{:S(2)}, u32[]{:S(2)}) collective-permute-start(bf16[1,2,256]{2,1,0:T(2,128)(2,1)S(1)} %get-tuple-element.16), channel_id=1, source_target_pairs={{0,3},{1,0},{2,1},{3,2},{4,7},{5,4},{6,5},{7,6},{8,11},{9,8},{10,9... | collective-permute-start | bytes 3080 | tf_op jit(solution)/shard_map/ppermute | solution.py:29
  9.8 7.4 %collective-permute-start.2 = (bf16[1,2,256]{2,1,0:T(2,128)(2,1)S(1)}, bf16[1,2,256]{2,1,0:T(2,128)(2,1)S(1)}, u32[]{:S(2)}, u32[]{:S(2)}) collective-permute-start(bf16[1,2,256]{2,1,0:T(2,128)(2,1)S(1)} %get-tuple-element.17), channel_id=1, source_target_pairs={{0,2},{1,3},{2,0},{3,1},{4,6},{5,7},{6,4},{7,5},{8,10},{9,11},{10,... | collective-permute-start | bytes 3080 | tf_op jit(solution)/shard_map/ppermute | solution.py:29
  9.8 7.4 %collective-permute-start.1 = (bf16[1,2,256]{2,1,0:T(2,128)(2,1)S(1)}, bf16[1,2,256]{2,1,0:T(2,128)(2,1)S(1)}, u32[]{:S(2)}, u32[]{:S(2)}) collective-permute-start(bf16[1,2,256]{2,1,0:T(2,128)(2,1)S(1)} %get-tuple-element.18), channel_id=1, source_target_pairs={{0,1},{1,2},{2,3},{3,0},{4,5},{5,6},{6,7},{7,4},{8,9},{9,10},{10,1... | collective-permute-start | bytes 3080 | tf_op jit(solution)/shard_map/ppermute | solution.py:29
  13.1 9.7 %all-to-all-start.4 = ((bf16[4,2,256]{2,1,0:T(2,128)(2,1)}), bf16[4,2,256]{2,1,0:T(2,128)(2,1)S(1)}, u32[]{:S(2)}, u32[]{:S(2)}) async-start(bf16[4,2,256]{2,1,0:T(2,128)(2,1)} %reshape.286), calls=%async_computation.4 | async-start | bytes 8192 | tf_op jit(solution)/shard_map/all_to_all | solution.py:149
  22.8 7.0 %all-to-all-start.6 = ((bf16[4,2,256]{2,1,0:T(2,128)(2,1)}), bf16[4,2,256]{2,1,0:T(2,128)(2,1)S(1)}, u32[]{:S(2)}, u32[]{:S(2)}) async-start(bf16[4,2,256]{2,1,0:T(2,128)(2,1)} %gather_fusion), calls=%async_computation.6 | async-start | bytes 8192 | tf_op jit(solution)/shard_map/all_to_all | solution.py:155
  29.8 7.6 %all-to-all-start.5 = ((bf16[4,2,256]{2,1,0:T(2,128)(2,1)}), bf16[4,2,256]{2,1,0:T(2,128)(2,1)S(1)}, u32[]{:S(2)}, u32[]{:S(2)}) async-start(bf16[4,2,256]{2,1,0:T(2,128)(2,1)} %all_to_all.80), calls=%async_computation.5 | async-start | bytes 8192 | tf_op jit(solution)/shard_map/all_to_all | solution.py:148
  37.4 19.6 %all-to-all-start.2 = ((bf16[1,8,256,128]{3,2,0,1:T(8,128)(2,1)}), bf16[1,8,256,128]{3,2,0,1:T(8,128)(2,1)}, u32[]{:S(2)}, u32[]{:S(2)}) async-start(bf16[1,8,256,128]{3,2,0,1:T(8,128)(2,1)} %fusion.15), calls=%async_computation.2 | async-start | bytes 1048576 | tf_op jit(solution)/shard_map/all_to_all | solution.py:142
  41.5 5.9 %copy-start.5 = (f32[4,1024]{1,0:T(4,128)S(1)}, f32[4,1024]{1,0:T(4,128)}, u32[]{:S(2)}) copy-start(f32[4,1024]{1,0:T(4,128)} %param.20) | copy-start | bytes 49156
  45.0 3.2 %collective-permute-start = (bf16[1,8,3,128]{3,2,1,0:T(4,128)(2,1)S(1)}, bf16[1,8,3,128]{3,2,1,0:T(4,128)(2,1)S(1)}, u32[]{:S(2)}, u32[]{:S(2)}) collective-permute-start(bf16[1,8,3,128]{3,2,1,0:T(4,128)(2,1)S(1)} %slice.50), channel_id=1, source_target_pairs={{0,4},{4,8},{8,12},{1,5},{5,9},{9,13},{2,6},{6,10},{10,14},{3,7},{... | collective-permute-start | bytes 18440 | tf_op jit(solution)/shard_map/ppermute | solution.py:37
  48.3 12.8 %copy-start.7 = (bf16[1,2,128]{2,1,0:T(2,128)(2,1)S(1)}, bf16[1,2,128]{2,1,0:T(2,128)(2,1)}, u32[]{:S(2)}) copy-start(bf16[1,2,128]{2,1,0:T(2,128)(2,1)} %param.23) | copy-start | bytes 1540
  48.3 12.8 %copy-start.11 = (bf16[1,2,128]{2,1,0:T(2,128)(2,1)S(1)}, bf16[1,2,128]{2,1,0:T(2,128)(2,1)}, u32[]{:S(2)}) copy-start(bf16[1,2,128]{2,1,0:T(2,128)(2,1)} %param.24) | copy-start | bytes 1540
  48.3 12.9 %copy-start.12 = (f32[1,2]{1,0:T(1,128)S(1)}, f32[1,2]{1,0:T(1,128)}, u32[]{:S(2)}) copy-start(f32[1,2]{1,0:T(1,128)} %param.27) | copy-start | bytes 28
  48.4 12.9 %copy-start.4 = (f32[1,2,1024]{2,1,0:T(2,128)S(1)}, f32[1,2,1024]{2,1,0:T(2,128)}, u32[]{:S(2)}) copy-start(f32[1,2,1024]{2,1,0:T(2,128)} %param.22) | copy-start | bytes 24580
  49.8 41.7 %copy-start.6 = (f32[1,2,1024]{2,1,0:T(2,128)S(1)}, f32[1,2,1024]{2,1,0:T(2,128)}, u32[]{:S(2)}) copy-start(f32[1,2,1024]{2,1,0:T(2,128)} %param.21) | copy-start | bytes 24580
  49.8 41.9 %copy-start.8 = (f32[1,2]{1,0:T(1,128)S(1)}, f32[1,2]{1,0:T(1,128)}, u32[]{:S(2)}) copy-start(f32[1,2]{1,0:T(1,128)} %param.26) | copy-start | bytes 28
  56.9 18.7 %all-to-all-start = ((bf16[1,8,256,128]{3,2,0,1:T(8,128)(2,1)}), bf16[1,8,256,128]{3,2,0,1:T(8,128)(2,1)}, u32[]{:S(2)}, u32[]{:S(2)}) async-start(bf16[1,8,256,128]{3,2,0,1:T(8,128)(2,1)} %fusion.30), calls=%async_computation | async-start | bytes 1048576 | tf_op jit(solution)/shard_map/all_to_all | solution.py:135
  75.7 12.3 %all-to-all-start.3 = ((bf16[4,2,256,128]{3,2,1,0:T(8,128)(2,1)}), bf16[4,2,256,128]{3,2,1,0:T(8,128)(2,1)S(1)}, u32[]{:S(2)}, u32[]{:S(2)}) async-start(bf16[4,2,256,128]{3,2,1,0:T(8,128)(2,1)} %bitcast.18), calls=%async_computation.3 | async-start | bytes 1048576 | tf_op jit(solution)/shard_map/all_to_all | solution.py:141
  87.9 13.7 %copy-start.9 = (bf16[1,2,128]{2,1,0:T(2,128)(2,1)S(1)}, bf16[1,2,128]{2,1,0:T(2,128)(2,1)}, u32[]{:S(2)}) copy-start(bf16[1,2,128]{2,1,0:T(2,128)(2,1)} %param.25) | copy-start | bytes 1540
  87.9 12.4 %all-to-all-start.1 = ((bf16[4,2,256,128]{3,2,1,0:T(8,128)(2,1)}), bf16[4,2,256,128]{3,2,1,0:T(8,128)(2,1)S(1)}, u32[]{:S(2)}, u32[]{:S(2)}) async-start(bf16[4,2,256,128]{3,2,1,0:T(8,128)(2,1)} %bitcast.10), calls=%async_computation.1 | async-start | bytes 1048576 | tf_op jit(solution)/shard_map/all_to_all | solution.py:134
  91.8 10.4 %copy-start.1 = (bf16[4,2,256,128]{3,2,0,1:T(8,128)(2,1)}, bf16[4,2,256,128]{3,2,0,1:T(8,128)(2,1)S(1)}, u32[]{:S(2)}) copy-start(bf16[4,2,256,128]{3,2,0,1:T(8,128)(2,1)S(1)} %copy.44) | copy-start | bytes 1572868
  100.4 1.9 %copy-start.2 = (bf16[4,2,256,128]{3,2,0,1:T(8,128)(2,1)}, bf16[4,2,256,128]{3,2,0,1:T(8,128)(2,1)S(1)}, u32[]{:S(2)}) copy-start(bf16[4,2,256,128]{3,2,0,1:T(8,128)(2,1)S(1)} %copy.41) | copy-start | bytes 1572868
